TPU v7x, 32 devices: a whole 2x2x4 slice. The times are simulated.
32 devices in a mesh: fs: 8 (over z, y), tp: 4 (over x, core).
Axes of the slice: x: 2, y: 2, z: 4, core: 2. Of those that a mesh axis runs over, the one named last changes fastest.
Arguments:
- layer_input: bfloat16 [16384, 2048], P('fs'), may hold values from -6 to 6
- input_cotangent: bfloat16 [16384, 2048], P('fs', 'tp'), may hold values from -6 to 6
- gate_cotangent: bfloat16 [16384, 2048], P('fs', 'tp'), may hold values from -6 to 6
- input_weight: float32 [2048, 2048], P('fs', 'tp'), may hold values from -0.125 to 0.125
- gate_weight: float32 [2048, 2048], P('fs', 'tp'), may hold values from -0.125 to 0.125
- input_basis: bfloat16 [2048, 256], P('fs'), may hold values from -1.81196113 to 1.81196113
- gate_basis: bfloat16 [2048, 256], P('fs'), may hold values from -1.81196113 to 1.81196113
- input_first: float32 [256, 2048], P('fs', 'tp'), may hold values from -10496 to 10496
- input_second: float32 [256, 2048], P('fs', 'tp'), may hold values from 16384 to 491520
- gate_first: float32 [256, 2048], P('fs', 'tp'), may hold values from -10496 to 10496
- gate_second: float32 [256, 2048], P('fs', 'tp'), may hold values from 16384 to 491520
Outputs:
- input_new: float32 [2048, 2048], P('fs', 'tp')
- gate_new: float32 [2048, 2048], P('fs', 'tp')
- input_step: float32 [2048, 2048], P('fs', 'tp')
- gate_step: float32 [2048, 2048], P('fs', 'tp')
- input_first_new: float32 [256, 2048], P('fs', 'tp')
- input_second_new: float32 [256, 2048], P('fs', 'tp')
- gate_first_new: float32 [256, 2048], P('fs', 'tp')
- gate_second_new: float32 [256, 2048], P('fs', 'tp')
- input_copy: bfloat16 [2048, 2048], P(None, 'tp')
- gate_copy: bfloat16 [2048, 2048], P(None, 'tp')
All inputs are finite; a program needn't handle non-finite values.
Results may differ from a plain program's by a relative error of at most 0.0055.
Values may be sent and summed in bfloat16 or wider, within the bound.
A program may use at most 64 MiB of HBM per device.

v0:
```python
import jax
import jax.numpy as jnp
from jax import lax
from jax.sharding import PartitionSpec as P

D = 2048
W = 2048
first_decay = 0.8
second_decay = 0.95
learn_rate = 0.01


def moments(small, first, second):
    first_new = first_decay * first + (1.0 - first_decay) * small
    second_new = second_decay * second + (1.0 - second_decay) * small * small
    direction = (first_new / (jnp.sqrt(second_new) + 1e-08)).astype(jnp.bfloat16)
    return (first_new, second_new, direction)


def split_product(projected, cotangent):
    upper = projected.astype(jnp.bfloat16)
    lower = (projected - upper.astype(jnp.float32)).astype(jnp.bfloat16)
    dims = (((0,), (0,)), ((), ()))
    return lax.dot_general(
        upper, cotangent, dims, preferred_element_type=jnp.float32
    ) + lax.dot_general(lower, cotangent, dims, preferred_element_type=jnp.float32)


def shards(
    layer_input,
    input_cotangent,
    gate_cotangent,
    input_weight,
    gate_weight,
    input_basis,
    gate_basis,
    input_first,
    input_second,
    gate_first,
    gate_second,
):
    pieces = (
        lax.all_gather(input_basis, "fs", axis=0, tiled=True),
        lax.all_gather(gate_basis, "fs", axis=0, tiled=True),
    )
    input_proj = jnp.dot(layer_input, pieces[0], preferred_element_type=jnp.float32)
    gate_proj = jnp.dot(layer_input, pieces[1], preferred_element_type=jnp.float32)
    input_small = split_product(input_proj, input_cotangent)
    gate_small = split_product(gate_proj, gate_cotangent)
    input_part, gate_part = (
        lax.psum_scatter(input_small, "fs", scatter_dimension=0, tiled=True),
        lax.psum_scatter(gate_small, "fs", scatter_dimension=0, tiled=True),
    )
    in_first, in_second, in_direction = moments(input_part, input_first, input_second)
    gt_first, gt_second, gt_direction = moments(gate_part, gate_first, gate_second)
    pieces = (
        lax.all_gather(in_direction, "fs", axis=0, tiled=True),
        lax.all_gather(gt_direction, "fs", axis=0, tiled=True),
    )
    input_update = jnp.dot(input_basis, pieces[0], preferred_element_type=jnp.float32)
    gate_update = jnp.dot(gate_basis, pieces[1], preferred_element_type=jnp.float32)
    input_squares, gate_squares = lax.psum(
        (jnp.sum(input_update * input_update), jnp.sum(gate_update * gate_update)), ("fs", "tp")
    )
    input_factor = jnp.minimum(1.0, 1.0 / jnp.sqrt(input_squares / (D * W) + 1e-06))
    gate_factor = jnp.minimum(1.0, 1.0 / jnp.sqrt(gate_squares / (D * W) + 1e-06))
    input_step = input_factor * input_update
    gate_step = gate_factor * gate_update
    input_new = input_weight - learn_rate * input_step
    gate_new = gate_weight - learn_rate * gate_step
    input_copy, gate_copy = (
        lax.all_gather(input_new.astype(jnp.bfloat16), "fs", axis=0, tiled=True),
        lax.all_gather(gate_new.astype(jnp.bfloat16), "fs", axis=0, tiled=True),
    )
    return (
        input_new,
        gate_new,
        input_step,
        gate_step,
        in_first,
        in_second,
        gt_first,
        gt_second,
        input_copy,
        gate_copy,
    )


def solution(mesh):
    placed = (
        P("fs", None),
        P("fs", "tp"),
        P("fs", "tp"),
        P("fs", "tp"),
        P("fs", "tp"),
        P("fs", None),
        P("fs", None),
        P("fs", "tp"),
        P("fs", "tp"),
        P("fs", "tp"),
        P("fs", "tp"),
    )
    return jax.shard_map(
        shards,
        mesh=mesh,
        in_specs=placed,
        out_specs=(
            P("fs", "tp"),
            P("fs", "tp"),
            P("fs", "tp"),
            P("fs", "tp"),
            P("fs", "tp"),
            P("fs", "tp"),
            P("fs", "tp"),
            P("fs", "tp"),
            P(None, "tp"),
            P(None, "tp"),
        ),
        check_vma=False,
    )
```

profile of v0, /device:TPU:0, one launch (start us, length us, event | category | flops | bytes accessed | tf_op | source)
XLA Modules:
  0.0 412.4 jit_solution(7743012523781812951)
XLA Ops:
  7.2 0.7 all-gather.7.cloned.1.call-update
  8.0 0.7 all-gather.5.cloned.1.call-update
  8.7 44.4 %all-gather.7.cloned.1.call-done = bf16[2048,256]{1,0:T(8,128)(2,1)} async-done(((bf16[256,256]{1,0:T(8,128)(2,1)}), bf16[2048,256]{1,0:T(8,128)(2,1)}) %all-gather.7.cloned.1.call-update) | async-done | bytes 1048592 | tf_op jit(solution)/shard_map/all_gather | solution.py:44
  53.2 6.1 %fusion.13 = f32[2048,256]{1,0:T(8,128)S(1)} fusion(bf16[2048,2048]{1,0:T(8,128)(2,1)} %param.11, bf16[2048,256]{1,0:T(8,128)(2,1)} %all-gather.7.cloned.1.call-done), kind=kOutput, calls=%fused_computation.27 | convolution fusion | flops 2147483648 | bytes 11534336 | tf_op jit(solution)/shard_map/dot_general | solution.py:47
  59.3 0.8 fusion.1
  60.0 1.6 convolution_add_fusion
  61.6 0.0 reduce-scatter.3.cloned.1.call-start
  61.7 32.6 %all-gather.5.cloned.1.call-done = bf16[2048,256]{1,0:T(8,128)(2,1)} async-done(((bf16[256,256]{1,0:T(8,128)(2,1)}), bf16[2048,256]{1,0:T(8,128)(2,1)}) %all-gather.5.cloned.1.call-update) | async-done | bytes 1048592 | tf_op jit(solution)/shard_map/all_gather | solution.py:43
  94.3 6.2 %fusion.12 = f32[2048,256]{1,0:T(8,128)S(1)} fusion(bf16[2048,2048]{1,0:T(8,128)(2,1)} %param.11, bf16[2048,256]{1,0:T(8,128)(2,1)} %all-gather.5.cloned.1.call-done), kind=kOutput, calls=%fused_computation.26 | convolution fusion | flops 2147483648 | bytes 11534336 | tf_op jit(solution)/shard_map/dot_general | solution.py:46
  100.6 0.7 fusion.4
  101.4 1.5 convolution_add_fusion.1
  103.0 1.0 copy.21
  104.0 55.7 %reduce-scatter.5.cloned.1.call-done = f32[32,512]{1,0:T(8,128)} async-done(((f32[256,512]{1,0:T(8,128)}), f32[32,512]{1,0:T(8,128)}) %reduce-scatter.5.cloned.1.call-update) | async-done | bytes 65552 | tf_op jit(solution)/shard_map/reduce_scatter | solution.py:52
  159.7 1.5 divide_convert_fusion
  161.3 30.9 %all_gather.21 = bf16[256,512]{1,0:T(8,128)(2,1)S(1)} all-gather(bf16[32,512]{1,0:T(8,128)(2,1)S(1)} %get-tuple-element.28), channel_id=1, replica_groups=mesh['fs'=8,'tp'=4] {'fs'}, dimensions={0}, use_global_device_ids=true | all-gather | bytes 294912 | tf_op jit(solution)/shard_map/all_gather | solution.py:58
  192.2 0.9 multiply_reduce_fusion
  193.1 32.0 %reduce-scatter.3.cloned.1.call-done = f32[32,512]{1,0:T(8,128)} async-done(((f32[256,512]{1,0:T(8,128)}), f32[32,512]{1,0:T(8,128)}) %reduce-scatter.3.cloned.1.call-update) | async-done | bytes 65552 | tf_op jit(solution)/shard_map/reduce_scatter | solution.py:51
  225.2 1.5 divide_convert_fusion.1
  226.7 30.8 %all_gather.19 = bf16[256,512]{1,0:T(8,128)(2,1)S(1)} all-gather(bf16[32,512]{1,0:T(8,128)(2,1)S(1)} %get-tuple-element.31), channel_id=1, replica_groups=mesh['fs'=8,'tp'=4] {'fs'}, dimensions={0}, use_global_device_ids=true | all-gather | bytes 294912 | tf_op jit(solution)/shard_map/all_gather | solution.py:57
  257.5 1.7 multiply_reduce_fusion.1
  259.2 37.8 %all-reduce = (f32[]{:T(128)}, f32[]{:T(128)}) all-reduce(f32[]{:T(128)} %get-tuple-element.34, f32[]{:T(128)} %get-tuple-element.36), channel_id=1, replica_groups=mesh['fs'=8,'tp'=4] {'fs','tp'}, use_global_device_ids=true, to_apply=%region_2.0 | all-reduce | flops 2 | bytes 16 | tf_op jit(solution)/shard_map/psum | solution.py:62
  297.7 2.2 fusion.9
  299.9 2.0 copy.22
  302.6 2.2 fusion.8
  304.9 2.1 copy.24
  307.0 2.1 copy.26
  309.0 1.0 copy.23
  310.0 1.0 copy.25
  311.0 40.2 %all-gather.9.cloned.1.call-done = bf16[2048,512]{0,1:T(8,128)(2,1)} async-done(((bf16[256,512]{0,1:T(8,128)(2,1)}), bf16[2048,512]{0,1:T(8,128)(2,1)}) %all-gather.9.cloned.1.call-update) | async-done | bytes 2097168 | tf_op jit(solution)/shard_map/all_gather | solution.py:72
  351.2 3.9 copy.27
  355.1 46.5 %all-gather.11.cloned.1.call-done = bf16[2048,512]{0,1:T(8,128)(2,1)} async-done(((bf16[256,512]{0,1:T(8,128)(2,1)}), bf16[2048,512]{0,1:T(8,128)(2,1)}) %all-gather.11.cloned.1.call-update) | async-done | bytes 2097168 | tf_op jit(solution)/shard_map/all_gather | solution.py:73
  401.7 3.9 copy.28
  (29 shorter events, 0.3 us)
Async XLA Ops:
  7.2 52.1 %copy-start = (bf16[2048,512]{1,0:T(8,128)(2,1)S(1)}, bf16[2048,512]{1,0:T(8,128)(2,1)}, u32[]{:S(2)}) copy-start(bf16[2048,512]{1,0:T(8,128)(2,1)} %param.13) | copy-start | bytes 6291460
  7.2 46.0 %all-gather.7.cloned.1.call-start = ((), (), s32[]{:S(2)}) async-start(), calls=%async_computation.4 | async-start | bytes 1179648 | tf_op jit(solution)/shard_map/all_gather | solution.py:44
  7.9 86.4 %all-gather.5.cloned.1.call-start = ((), (), s32[]{:S(2)}) async-start(), calls=%async_computation.2 | async-start | bytes 1179648 | tf_op jit(solution)/shard_map/all_gather | solution.py:43
  8.7 151.1 %reduce-scatter.5.cloned.1.call-start = ((), (), s32[]{:S(2)}) async-start(), calls=%async_computation.5 | async-start | bytes 589824 | tf_op jit(solution)/shard_map/reduce_scatter | solution.py:52
  61.6 163.5 %reduce-scatter.3.cloned.1.call-start = ((), (), s32[]{:S(2)}) async-start(), calls=%async_computation.3 | async-start | bytes 589824 | tf_op jit(solution)/shard_map/reduce_scatter | solution.py:51
  94.3 6.2 %copy-start.1 = (bf16[2048,512]{1,0:T(8,128)(2,1)S(1)}, bf16[2048,512]{1,0:T(8,128)(2,1)}, u32[]{:S(2)}) copy-start(bf16[2048,512]{1,0:T(8,128)(2,1)} %param.12) | copy-start | bytes 6291460
  101.3 1.7 copy-start.5
  101.3 58.4 %copy-start.6 = (f32[32,512]{1,0:T(8,128)S(1)}, f32[32,512]{1,0:T(8,128)}, u32[]{:S(2)}) copy-start(f32[32,512]{1,0:T(8,128)} %param.21) | copy-start | bytes 196612
  101.4 58.4 %copy-start.7 = (f32[32,512]{1,0:T(8,128)S(1)}, f32[32,512]{1,0:T(8,128)}, u32[]{:S(2)}) copy-start(f32[32,512]{1,0:T(8,128)} %param.20) | copy-start | bytes 196612
  102.9 89.3 %copy-start.3 = (bf16[256,256]{1,0:T(8,128)(2,1)S(1)}, bf16[256,256]{1,0:T(8,128)(2,1)}, u32[]{:S(2)}) copy-start(bf16[256,256]{1,0:T(8,128)(2,1)} %param.17) | copy-start | bytes 393220
  102.9 122.3 %copy-start.8 = (f32[32,512]{1,0:T(8,128)S(1)}, f32[32,512]{1,0:T(8,128)}, u32[]{:S(2)}) copy-start(f32[32,512]{1,0:T(8,128)} %param.19) | copy-start | bytes 196612
  102.9 122.3 %copy-start.9 = (f32[32,512]{1,0:T(8,128)S(1)}, f32[32,512]{1,0:T(8,128)}, u32[]{:S(2)}) copy-start(f32[32,512]{1,0:T(8,128)} %param.18) | copy-start | bytes 196612
  102.9 154.6 %copy-start.4 = (bf16[256,256]{1,0:T(8,128)(2,1)S(1)}, bf16[256,256]{1,0:T(8,128)(2,1)}, u32[]{:S(2)}) copy-start(bf16[256,256]{1,0:T(8,128)(2,1)} %param.16) | copy-start | bytes 393220
  102.9 248.3 %all-gather.9.cloned.1.call-start = ((), (), s32[]{:S(2)}) async-start(), calls=%async_computation.6 | async-start | bytes 2359296 | tf_op jit(solution)/shard_map/all_gather | solution.py:72
  299.9 101.8 %all-gather.11.cloned.1.call-start = ((), (), s32[]{:S(2)}) async-start(), calls=%async_computation.7 | async-start | bytes 2359296 | tf_op jit(solution)/shard_map/all_gather | solution.py:73
  304.9 4.2 %copy-start.2 = (f32[256,512]{0,1:T(8,128)S(1)}, f32[256,512]{0,1:T(8,128)}, u32[]{:S(2)}) copy-start(f32[256,512]{0,1:T(8,128)} %get-tuple-element.26) | copy-start | bytes 1572868
Sparse Core Ops, SparseCore 0:
  10.1 42.9 all-gather.6
  55.3 39.0 all-gather.4
  98.3 61.4 reduce-scatter.4
  163.5 61.6 reduce-scatter.2
  300.0 51.1 all-gather.8
  353.1 48.5 all-gather.10
where the time goes:
time: 413 us; the launch traced here: 412 us
  waiting for transfers between devices  253 us (61%)
  blocking collectives  99.5 us (24%)
  matrix products  19.5 us (5%)
  local copies, waits for them, and re-layouts  17.1 us (4%)
  between operations  15.6 us (4%)
  other arithmetic  7.44 us (2%)
    reduce_scatter x1, waiting for transfers between devices, shards(): lax.psum_scatter(gate_small, 'fs', scatter_dimension=0, tiled=True)  55.7 us
    all_gather x1, waiting for transfers between devices, shards(): lax.all_gather(gate_new.astype(jnp.bfloat16), 'fs', axis=0, tiled=True)  46.5 us
    all_gather x1, waiting for transfers between devices, shards(): lax.all_gather(gate_basis, 'fs', axis=0, tiled=True)  44.4 us
    all_gather x1, waiting for transfers between devices, shards(): lax.all_gather(input_new.astype(jnp.bfloat16), 'fs', axis=0, tiled=True)  40.2 us
    psum x1, blocking collectives, shards(): lax.psum((jnp.sum(input_update * input_update), jnp.sum(gate_update * gat...  37.8 us
    all_gather x1, waiting for transfers between devices, shards(): lax.all_gather(input_basis, 'fs', axis=0, tiled=True)  32.6 us
    reduce_scatter x1, waiting for transfers between devices, shards(): lax.psum_scatter(input_small, 'fs', scatter_dimension=0, tiled=True)  32 us
    all_gather x1, blocking collectives, shards(): lax.all_gather(gt_direction, 'fs', axis=0, tiled=True)  30.9 us
  transfers between devices with their start and end apart: 6, of which 6 were waited for; matrix products, arithmetic and copies ran while one was open for 8% of the time, Pallas kernels for 0%

commit v1 on v0

--- a/solution.py
+++ b/solution.py
@@ -1,13 +1,24 @@
+import functools
 import jax
 import jax.numpy as jnp
 from jax import lax
 from jax.sharding import PartitionSpec as P
+from jax.lax import psum
 
 D = 2048
 W = 2048
 first_decay = 0.8
 second_decay = 0.95
 learn_rate = 0.01
+
+
+def choose_outputs_now(u, mesh_name, axis_name):
+    for jj in (mesh_name, axis_name):
+        u = psum(u, jj)
+    return u
+
+
+play_trees_now = functools.partial(choose_outputs_now, mesh_name="tp", axis_name="fs")
 
 
 def moments(small, first, second):
@@ -59,8 +70,8 @@
     )
     input_update = jnp.dot(input_basis, pieces[0], preferred_element_type=jnp.float32)
     gate_update = jnp.dot(gate_basis, pieces[1], preferred_element_type=jnp.float32)
-    input_squares, gate_squares = lax.psum(
-        (jnp.sum(input_update * input_update), jnp.sum(gate_update * gate_update)), ("fs", "tp")
+    input_squares, gate_squares = play_trees_now(
+        (jnp.sum(input_update * input_update), jnp.sum(gate_update * gate_update))
     )
     input_factor = jnp.minimum(1.0, 1.0 / jnp.sqrt(input_squares / (D * W) + 1e-06))
     gate_factor = jnp.minimum(1.0, 1.0 / jnp.sqrt(gate_squares / (D * W) + 1e-06))

time: 413 us -> 398 us (0.964)
  blocking collectives: 99.5 us -> 88.1 us
    psum x1 -> x2, blocking collectives: 37.8 us -> 26.2 us  [choose_outputs_now(): u = psum(u, jj)]
    unnamed x28 -> x26, local copies, waits for them, and re-layouts: 17.1 us -> 16.2 us
  transfers between devices with their start and end apart: 6 -> 6, of which waited for: 6 -> 6; matrix products, arithmetic and copies ran while one was open for 8% -> 9% of each run, Pallas kernels for 0% -> 0%
where the time goes in v1:
time: 398 us; the launch traced here: 397 us
  waiting for transfers between devices  250 us (63%)
  blocking collectives  88.1 us (22%)
  matrix products  19.5 us (5%)
  local copies, waits for them, and re-layouts  16.2 us (4%)
  between operations  15.6 us (4%)
  other arithmetic  7.55 us (2%)
    reduce_scatter x1, waiting for transfers between devices, shards(): lax.psum_scatter(gate_small, 'fs', scatter_dimension=0, tiled=True)  56.5 us
    all_gather x1, waiting for transfers between devices, shards(): lax.all_gather(gate_new.astype(jnp.bfloat16), 'fs', axis=0, tiled=True)  46.5 us
    all_gather x1, waiting for transfers between devices, shards(): lax.all_gather(gate_basis, 'fs', axis=0, tiled=True)  44.4 us
    all_gather x1, waiting for transfers between devices, shards(): lax.all_gather(input_new.astype(jnp.bfloat16), 'fs', axis=0, tiled=True)  36.4 us
    all_gather x1, waiting for transfers between devices, shards(): lax.all_gather(input_basis, 'fs', axis=0, tiled=True)  32.6 us
    reduce_scatter x1, waiting for transfers between devices, shards(): lax.psum_scatter(input_small, 'fs', scatter_dimension=0, tiled=True)  32 us
    all_gather x1, blocking collectives, shards(): lax.all_gather(gt_direction, 'fs', axis=0, tiled=True)  31 us
    all_gather x1, blocking collectives, shards(): lax.all_gather(in_direction, 'fs', axis=0, tiled=True)  30.9 us
  transfers between devices with their start and end apart: 6, of which 6 were waited for; matrix products, arithmetic and copies ran while one was open for 9% of the time, Pallas kernels for 0%

profile of v1, /device:TPU:0, one launch (start us, length us, event | category | flops | bytes accessed | tf_op | source)
XLA Modules:
  0.0 397.4 jit_solution(8143283661222558773)
XLA Ops:
  7.2 0.7 all-gather.7.cloned.1.call-update
  8.0 0.7 all-gather.5.cloned.1.call-update
  8.7 44.4 %all-gather.7.cloned.1.call-done = bf16[2048,256]{1,0:T(8,128)(2,1)} async-done(((bf16[256,256]{1,0:T(8,128)(2,1)}), bf16[2048,256]{1,0:T(8,128)(2,1)}) %all-gather.7.cloned.1.call-update) | async-done | bytes 1048592 | tf_op jit(solution)/shard_map/all_gather | solution.py:55
  53.2 6.1 %fusion.13 = f32[2048,256]{1,0:T(8,128)S(1)} fusion(bf16[2048,2048]{1,0:T(8,128)(2,1)} %param.11, bf16[2048,256]{1,0:T(8,128)(2,1)} %all-gather.7.cloned.1.call-done), kind=kOutput, calls=%fused_computation.27 | convolution fusion | flops 2147483648 | bytes 11534336 | tf_op jit(solution)/shard_map/dot_general | solution.py:58
  59.3 0.8 fusion.1
  60.0 1.6 convolution_add_fusion
  61.7 32.6 %all-gather.5.cloned.1.call-done = bf16[2048,256]{1,0:T(8,128)(2,1)} async-done(((bf16[256,256]{1,0:T(8,128)(2,1)}), bf16[2048,256]{1,0:T(8,128)(2,1)}) %all-gather.5.cloned.1.call-update) | async-done | bytes 1048592 | tf_op jit(solution)/shard_map/all_gather | solution.py:54
  94.3 6.2 %fusion.12 = f32[2048,256]{1,0:T(8,128)S(1)} fusion(bf16[2048,2048]{1,0:T(8,128)(2,1)} %param.11, bf16[2048,256]{1,0:T(8,128)(2,1)} %all-gather.5.cloned.1.call-done), kind=kOutput, calls=%fused_computation.26 | convolution fusion | flops 2147483648 | bytes 11534336 | tf_op jit(solution)/shard_map/dot_general | solution.py:57
  100.6 0.7 fusion.4
  101.4 1.5 convolution_add_fusion.1
  103.0 0.2 copy.21
  103.2 56.5 %reduce-scatter.5.cloned.1.call-done = f32[32,512]{1,0:T(8,128)} async-done(((f32[256,512]{1,0:T(8,128)}), f32[32,512]{1,0:T(8,128)}) %reduce-scatter.5.cloned.1.call-update) | async-done | bytes 65552 | tf_op jit(solution)/shard_map/reduce_scatter | solution.py:63
  159.7 1.5 divide_convert_fusion
  161.3 31.0 %all_gather.21 = bf16[256,512]{1,0:T(8,128)(2,1)S(1)} all-gather(bf16[32,512]{1,0:T(8,128)(2,1)S(1)} %get-tuple-element.30), channel_id=1, replica_groups=mesh['fs'=8,'tp'=4] {'fs'}, dimensions={0}, use_global_device_ids=true | all-gather | bytes 294912 | tf_op jit(solution)/shard_map/all_gather | solution.py:69
  192.3 0.9 multiply_reduce_fusion
  193.2 32.0 %reduce-scatter.3.cloned.1.call-done = f32[32,512]{1,0:T(8,128)} async-done(((f32[256,512]{1,0:T(8,128)}), f32[32,512]{1,0:T(8,128)}) %reduce-scatter.3.cloned.1.call-update) | async-done | bytes 65552 | tf_op jit(solution)/shard_map/reduce_scatter | solution.py:62
  225.2 1.6 divide_convert_fusion.1
  226.8 30.9 %all_gather.19 = bf16[256,512]{1,0:T(8,128)(2,1)S(1)} all-gather(bf16[32,512]{1,0:T(8,128)(2,1)S(1)} %get-tuple-element.33), channel_id=1, replica_groups=mesh['fs'=8,'tp'=4] {'fs'}, dimensions={0}, use_global_device_ids=true | all-gather | bytes 294912 | tf_op jit(solution)/shard_map/all_gather | solution.py:68
  257.7 1.7 multiply_reduce_fusion.1
  259.3 6.3 %all-reduce.1 = (f32[]{:T(128)}, f32[]{:T(128)}) all-reduce(f32[]{:T(128)} %get-tuple-element.36, f32[]{:T(128)} %get-tuple-element.38), channel_id=1, replica_groups=mesh['fs'=8,'tp'=4] {'tp'}, use_global_device_ids=true, to_apply=%region_2.0 | all-reduce | flops 2 | bytes 16 | tf_op jit(solution)/shard_map/psum | solution.py:17
  265.6 20.0 %all-reduce = (f32[]{:T(128)}, f32[]{:T(128)}) all-reduce(f32[]{:T(128)} %get-tuple-element.22, f32[]{:T(128)} %get-tuple-element.23), channel_id=1, replica_groups=mesh['fs'=8,'tp'=4] {'fs'}, use_global_device_ids=true, to_apply=%region_3.0 | all-reduce | flops 2 | bytes 16 | tf_op jit(solution)/shard_map/psum | solution.py:17
  286.3 2.2 fusion.9
  288.5 2.0 copy.22
  291.3 2.3 fusion.8
  293.6 2.1 copy.24
  295.7 2.0 copy.26
  297.7 1.0 copy.23
  298.7 1.0 copy.25
  299.7 36.4 %all-gather.9.cloned.1.call-done = bf16[2048,512]{0,1:T(8,128)(2,1)} async-done(((bf16[256,512]{0,1:T(8,128)(2,1)}), bf16[2048,512]{0,1:T(8,128)(2,1)}) %all-gather.9.cloned.1.call-update) | async-done | bytes 2097168 | tf_op jit(solution)/shard_map/all_gather | solution.py:83
  336.1 3.9 copy.27
  340.1 46.5 %all-gather.11.cloned.1.call-done = bf16[2048,512]{0,1:T(8,128)(2,1)} async-done(((bf16[256,512]{0,1:T(8,128)(2,1)}), bf16[2048,512]{0,1:T(8,128)(2,1)}) %all-gather.11.cloned.1.call-update) | async-done | bytes 2097168 | tf_op jit(solution)/shard_map/all_gather | solution.py:84
  386.6 3.9 copy.28
  (28 shorter events, 0.4 us)
Async XLA Ops:
  7.2 52.1 %copy-start = (bf16[2048,512]{1,0:T(8,128)(2,1)S(1)}, bf16[2048,512]{1,0:T(8,128)(2,1)}, u32[]{:S(2)}) copy-start(bf16[2048,512]{1,0:T(8,128)(2,1)} %param.13) | copy-start | bytes 6291460
  7.2 46.0 %all-gather.7.cloned.1.call-start = ((), (), s32[]{:S(2)}) async-start(), calls=%async_computation.4 | async-start | bytes 1179648 | tf_op jit(solution)/shard_map/all_gather | solution.py:55
  7.9 86.4 %all-gather.5.cloned.1.call-start = ((), (), s32[]{:S(2)}) async-start(), calls=%async_computation.2 | async-start | bytes 1179648 | tf_op jit(solution)/shard_map/all_gather | solution.py:54
  8.7 151.1 %reduce-scatter.5.cloned.1.call-start = ((), (), s32[]{:S(2)}) async-start(), calls=%async_computation.5 | async-start | bytes 589824 | tf_op jit(solution)/shard_map/reduce_scatter | solution.py:63
  61.6 163.6 %reduce-scatter.3.cloned.1.call-start = ((), (), s32[]{:S(2)}) async-start(), calls=%async_computation.3 | async-start | bytes 589824 | tf_op jit(solution)/shard_map/reduce_scatter | solution.py:62
  94.3 6.2 %copy-start.1 = (bf16[2048,512]{1,0:T(8,128)(2,1)S(1)}, bf16[2048,512]{1,0:T(8,128)(2,1)}, u32[]{:S(2)}) copy-start(bf16[2048,512]{1,0:T(8,128)(2,1)} %param.12) | copy-start | bytes 6291460
  101.3 1.6 copy-start.6
  101.3 58.4 %copy-start.7 = (f32[32,512]{1,0:T(8,128)S(1)}, f32[32,512]{1,0:T(8,128)}, u32[]{:S(2)}) copy-start(f32[32,512]{1,0:T(8,128)} %param.21) | copy-start | bytes 196612
  101.4 58.4 %copy-start.8 = (f32[32,512]{1,0:T(8,128)S(1)}, f32[32,512]{1,0:T(8,128)}, u32[]{:S(2)}) copy-start(f32[32,512]{1,0:T(8,128)} %param.20) | copy-start | bytes 196612
  102.9 89.4 %copy-start.4 = (bf16[256,256]{1,0:T(8,128)(2,1)S(1)}, bf16[256,256]{1,0:T(8,128)(2,1)}, u32[]{:S(2)}) copy-start(bf16[256,256]{1,0:T(8,128)(2,1)} %param.17) | copy-start | bytes 393220
  102.9 154.8 %copy-start.5 = (bf16[256,256]{1,0:T(8,128)(2,1)S(1)}, bf16[256,256]{1,0:T(8,128)(2,1)}, u32[]{:S(2)}) copy-start(bf16[256,256]{1,0:T(8,128)(2,1)} %param.16) | copy-start | bytes 393220
  102.9 233.2 %all-gather.9.cloned.1.call-start = ((), (), s32[]{:S(2)}) async-start(), calls=%async_computation.6 | async-start | bytes 2359296 | tf_op jit(solution)/shard_map/all_gather | solution.py:83
  288.5 98.1 %all-gather.11.cloned.1.call-start = ((), (), s32[]{:S(2)}) async-start(), calls=%async_computation.7 | async-start | bytes 2359296 | tf_op jit(solution)/shard_map/all_gather | solution.py:84
  291.3 6.4 %copy-start.3 = (f32[256,512]{0,1:T(8,128)S(1)}, f32[256,512]{0,1:T(8,128)}, u32[]{:S(2)}) copy-start(f32[256,512]{0,1:T(8,128)} %get-tuple-element.28) | copy-start | bytes 1572868
  293.5 5.2 %copy-start.2 = (f32[256,512]{0,1:T(8,128)S(1)}, f32[256,512]{0,1:T(8,128)}, u32[]{:S(2)}) copy-start(f32[256,512]{0,1:T(8,128)} %get-tuple-element.29) | copy-start | bytes 1572868
Sparse Core Ops, SparseCore 0:
  10.1 42.9 all-gather.6
  55.3 39.0 all-gather.4
  98.3 61.4 reduce-scatter.4
  163.5 61.6 reduce-scatter.2
  288.6 47.4 all-gather.8
  338.0 48.5 all-gather.10
